TPU v7x, 512 devices: a whole 4x4x16 slice. The times are simulated.
512 devices in a mesh: kv: 64 (over z, y), tp: 8 (over x, core).
Axes of the slice: x: 4, y: 4, z: 16, core: 2. Of those that a mesh axis runs over, the one named last changes fastest.
Arguments:
- queries: bfloat16 [16384, 1024], P('kv', 'tp'), may hold values from -4 to 4
- keys: bfloat16 [16384, 1024], P('kv', 'tp'), may hold values from -4 to 4
- values: bfloat16 [16384, 1024], P('kv', 'tp'), may hold values from -5 to 5
- log_sums: float32 [16, 16384], P('tp', 'kv'), may hold values from 5.5 to 7
- out_grad: bfloat16 [16384, 1024], P('kv', 'tp'), may hold values from -24 to 24
- chosen: int32 [128, 8], P('kv'), may hold values from -1 to 511, as said below
- normed: bfloat16 [16384, 2048], P('kv', 'tp'), may hold values from -0.23925781 to 0.23925781
Outputs:
- query_grad: bfloat16 [16384, 1024], P('kv', 'tp')
- key_grad: bfloat16 [16384, 1024], P('kv', 'tp')
- value_grad: bfloat16 [16384, 1024], P('kv', 'tp')
- weight_grad: float32 [2048, 1024], P('kv', 'tp')
Inputs may be any that keep to these rules, and one draw needn't show every extreme that they name: `chosen`: each used entry names a key block that ends at or before its query block's start; the used entries of one list are distinct. Among the lists of the 2 query blocks of one index of kv, the key blocks of any other index of kv appear as at most one distinct block; for every index from 1 on, the first query block's list names a block of the index before, and the last index's first query block's list names a block of index 0. Blocks of the own index of kv before the query block may appear freely.
All inputs are finite; a program needn't handle non-finite values.
Results may differ from a plain program's by a relative error of at most 0.008.
Values may be sent and summed in bfloat16 or wider, within the bound.
No kernel may reach another device: no remote copies, remote signals or barrier semaphores. Data moves between devices by JAX's collectives and lax.ppermute only.
A program may use at most 64 MiB of HBM per device.

v0:
```python
from functools import partial

import jax
import jax.numpy as jnp
from jax import lax
from jax.sharding import PartitionSpec as P

QB = 128
KB = 32


def in_one_piece(arrays, axis, split_dim, concat_dim, along):
    widths = [a.shape[along] for a in arrays]
    both = jnp.concatenate(arrays, axis=along)
    out = lax.all_to_all(both, axis, split_axis=split_dim, concat_axis=concat_dim, tiled=True)
    return tuple(jnp.split(out, [sum(widths[:k]) for k in range(1, len(widths))], axis=along))


def from_everyone(value, axis):
    count = lax.axis_size(axis)
    return lax.all_to_all(
        jnp.broadcast_to(value[None], (count, *value.shape)), axis, 0, 0, tiled=True
    )


def laid_out(blocks, dim):
    blocks = jnp.moveaxis(blocks, 0, dim)
    shape = blocks.shape
    return blocks.reshape(*shape[:dim], shape[dim] * shape[dim + 1], *shape[dim + 2 :])


def gathered_copies(value, axis, dim):
    blocks = from_everyone(value, axis)
    return laid_out(blocks, dim)


def in_blocks(value, dim, count):
    shape = value.shape
    blocks = value.reshape(*shape[:dim], count, shape[dim] // count, *shape[dim + 1 :])
    return jnp.moveaxis(blocks, dim, 0)


def sum_at_owner(value, axis, dim):
    blocks = in_blocks(value, dim, lax.axis_size(axis))
    arrived = lax.all_to_all(blocks, axis, split_axis=0, concat_axis=0, tiled=True)
    return arrived.astype(jnp.float32).sum(axis=0)


def block_grads(inputs, scaling):
    query_blk, grad_blk, sums_blk, keys_sel, vals_sel, keys_own, vals_own, eligible_blocks = inputs
    span_rows = query_blk.shape[0]
    scores = (
        jnp.einsum("qhd,skhd->hqsk", query_blk, keys_sel, preferred_element_type=jnp.float32)
        * scaling
    )
    weights = jnp.where(
        eligible_blocks[None, None, :, None], jnp.exp(scores - sums_blk[:, :, None, None]), 0.0
    )
    causal = lax.broadcasted_iota(jnp.int32, (span_rows, span_rows), 0) >= lax.broadcasted_iota(
        jnp.int32, (span_rows, span_rows), 1
    )
    own_scores = (
        jnp.einsum("qhd,khd->hqk", query_blk, keys_own, preferred_element_type=jnp.float32)
        * scaling
    )
    own_weights = jnp.where(causal[None], jnp.exp(own_scores - sums_blk[:, :, None]), 0.0)
    weights_low = weights.astype(jnp.bfloat16)
    own_low = own_weights.astype(jnp.bfloat16)
    attended = jnp.einsum(
        "hqsk,skhd->qhd", weights_low, vals_sel, preferred_element_type=jnp.float32
    )
    attended = attended + jnp.einsum(
        "hqk,khd->qhd", own_low, vals_own, preferred_element_type=jnp.float32
    )
    deltas = jnp.sum(grad_blk.astype(jnp.float32) * attended, axis=-1).T
    dots_sel = jnp.einsum("qhd,skhd->hqsk", grad_blk, vals_sel, preferred_element_type=jnp.float32)
    own_dots = jnp.einsum("qhd,khd->hqk", grad_blk, vals_own, preferred_element_type=jnp.float32)
    slopes = (weights * (dots_sel - deltas[:, :, None, None])).astype(jnp.bfloat16)
    own_slopes = (own_weights * (own_dots - deltas[:, :, None])).astype(jnp.bfloat16)
    query_part = jnp.einsum("hqsk,skhd->qhd", slopes, keys_sel, preferred_element_type=jnp.float32)
    query_part = scaling * (
        query_part
        + jnp.einsum("hqk,khd->qhd", own_slopes, keys_own, preferred_element_type=jnp.float32)
    )
    key_terms = scaling * jnp.einsum(
        "hqsk,qhd->skhd", slopes, query_blk, preferred_element_type=jnp.float32
    )
    value_terms = jnp.einsum(
        "hqsk,qhd->skhd", weights_low, grad_blk, preferred_element_type=jnp.float32
    )
    own_key_terms = scaling * jnp.einsum(
        "hqk,qhd->khd", own_slopes, query_blk, preferred_element_type=jnp.float32
    )
    own_value_terms = jnp.einsum(
        "hqk,qhd->khd", own_low, grad_blk, preferred_element_type=jnp.float32
    )
    return (query_part.astype(jnp.bfloat16), key_terms, value_terms, own_key_terms, own_value_terms)


def body(queries, keys, values, log_sums, out_grad, chosen, normed):
    devices = lax.axis_size("kv")
    myself = lax.axis_index("kv")
    rows_here, columns = queries.shape
    head_count = log_sums.shape[0]
    head_size = columns // head_count
    query_blocks = rows_here // QB
    key_blocks = rows_here // KB
    selected = chosen.shape[1]
    groups = 1
    slot_count = devices * groups
    owners = chosen // key_blocks
    offsets = chosen % key_blocks
    eligible_blocks = chosen >= 0
    remote = eligible_blocks & (owners != myself)
    slot_ids = owners * groups
    matches = remote[:, :, None] & (
        slot_ids[:, :, None] == jnp.arange(slot_count, dtype=jnp.int32)[None, None, :]
    )
    wanted = jnp.max(jnp.where(matches, offsets[:, :, None] + 1, 0), axis=(0, 1))
    requested = lax.all_to_all(
        wanted.reshape(devices, groups), "kv", split_axis=0, concat_axis=0, tiled=True
    ).reshape(-1)
    live_request = requested > 0
    picked = jnp.clip(requested - 1, 0, key_blocks - 1)
    key_table = keys.reshape(key_blocks, KB, columns)
    value_table = values.reshape(key_blocks, KB, columns)
    zero_block = jnp.zeros((), keys.dtype)
    outgoing_keys = jnp.where(live_request[:, None, None], key_table[picked], zero_block).reshape(
        devices, groups, KB, columns
    )
    outgoing_values = jnp.where(
        live_request[:, None, None], value_table[picked], zero_block
    ).reshape(devices, groups, KB, columns)
    fetched_keys, fetched_values = in_one_piece((outgoing_keys, outgoing_values), "kv", 0, 0, 1)
    all_keys = jnp.concatenate([fetched_keys.reshape(slot_count, KB, columns), key_table], axis=0)
    all_values = jnp.concatenate(
        [fetched_values.reshape(slot_count, KB, columns), value_table], axis=0
    )
    table_ids = jnp.where(remote, slot_ids, jnp.where(eligible_blocks, slot_count + offsets, 0))
    keys_sel = all_keys[table_ids].reshape(query_blocks, selected, KB, head_count, head_size)
    vals_sel = all_values[table_ids].reshape(query_blocks, selected, KB, head_count, head_size)
    block_shape = (query_blocks, QB, head_count, head_size)
    inputs = (
        queries.reshape(block_shape),
        out_grad.reshape(block_shape),
        log_sums.reshape(head_count, query_blocks, QB).transpose(1, 0, 2),
        keys_sel,
        vals_sel,
        keys.reshape(block_shape),
        values.reshape(block_shape),
        eligible_blocks,
    )
    query_part, key_terms, value_terms, own_key_terms, own_value_terms = lax.map(
        partial(block_grads, scaling=head_size ** (-0.5)), inputs
    )
    routes = (
        table_ids.reshape(-1)[:, None]
        == jnp.arange(slot_count + key_blocks, dtype=jnp.int32)[None, :]
    ) & eligible_blocks.reshape(-1)[:, None]
    stacked_terms = jnp.stack(
        [key_terms.reshape(-1, KB * columns), value_terms.reshape(-1, KB * columns)]
    )
    routed = jnp.einsum(
        "ab,xac->xbc", routes.astype(jnp.float32), stacked_terms, precision=lax.Precision.HIGHEST
    )
    back_keys = routed[0, :slot_count].reshape(devices, groups, KB, columns)
    back_values = routed[1, :slot_count].reshape(devices, groups, KB, columns)
    returned_keys, returned_values = tuple(
        (
            part.astype(jnp.float32)
            for part in in_one_piece(
                (back_keys.astype(jnp.bfloat16), back_values.astype(jnp.bfloat16)), "kv", 0, 0, 1
            )
        )
    )
    matched = (
        ((requested - 1)[:, None] == jnp.arange(key_blocks, dtype=jnp.int32)[None, :])
        & live_request[:, None]
    ).astype(jnp.float32)
    stacked_back = jnp.stack(
        [
            returned_keys.reshape(slot_count, KB * columns),
            returned_values.reshape(slot_count, KB * columns),
        ]
    )
    arrived = jnp.einsum("ab,xac->xbc", matched, stacked_back, precision=lax.Precision.HIGHEST)
    totals = arrived + routed[:, slot_count:]
    key_grad = (
        totals[0].reshape(rows_here, columns) + own_key_terms.reshape(rows_here, columns)
    ).astype(jnp.bfloat16)
    value_grad = (
        totals[1].reshape(rows_here, columns) + own_value_terms.reshape(rows_here, columns)
    ).astype(jnp.bfloat16)
    features_all = gathered_copies(normed, "tp", 1)
    weight_grad = sum_at_owner(
        lax.dot_general(
            features_all, value_grad, (((0,), (0,)), ((), ())), preferred_element_type=jnp.float32
        ).astype(jnp.bfloat16),
        "kv",
        0,
    )
    return (query_part.reshape(rows_here, columns), key_grad, value_grad, weight_grad)


def solution(mesh):
    in_specs = (
        P("kv", "tp"),
        P("kv", "tp"),
        P("kv", "tp"),
        P("tp", "kv"),
        P("kv", "tp"),
        P("kv", None),
        P("kv", "tp"),
    )
    out_specs = (P("kv", "tp"), P("kv", "tp"), P("kv", "tp"), P("kv", "tp"))
    return jax.shard_map(body, mesh=mesh, in_specs=in_specs, out_specs=out_specs, check_vma=False)
```

profile of v0, /device:TPU:8, one launch (start us, length us, event | category | flops | bytes accessed | tf_op | source)
XLA Modules:
  0.0 239.2 jit_solution(10323939308479358087)
XLA Ops:
  0.6 0.7 compare_select_fusion
  1.5 32.3 %all_to_all.29 = s32[64,1,1]{2,1,0:T(1,128)S(1)} all-to-all(s32[64,1,1]{2,1,0:T(1,128)S(1)} %copy.92), channel_id=1, replica_groups=mesh['kv'=64,'tp'=8] {'kv'}, dimensions={0} | all-to-all | bytes 512 | tf_op jit(solution)/shard_map/all_to_all | solution.py:120
  33.9 2.4 add_reduce_fusion
  36.3 1.5 gather_fusion
  37.8 1.5 gather_fusion.1
  39.3 1.2 compare_reduce_fusion
  40.5 0.2 bitcast_select_fusion.1
  40.7 1.1 pad_maximum_fusion
  41.8 5.3 %all-to-all-start.1 = ((bf16[64,2,32,128]{3,2,1,0:T(8,128)(2,1)}), bf16[64,2,32,128]{3,2,1,0:T(8,128)(2,1)S(1)}, u32[]{:S(2)}, u32[]{:S(2)}) async-start(bf16[64,2,32,128]{3,2,1,0:T(8,128)(2,1)} %pad_maximum_fusion), calls=%async_computation.1 | async-start | bytes 2097152 | tf_op jit(solution)/shard_map/all_to_all | solution.py:15
  48.3 53.0 %all-to-all-done.1 = bf16[64,2,32,128]{3,2,1,0:T(8,128)(2,1)S(1)} async-done(((bf16[64,2,32,128]{3,2,1,0:T(8,128)(2,1)}), bf16[64,2,32,128]{3,2,1,0:T(8,128)(2,1)S(1)}, u32[]{:S(2)}, u32[]{:S(2)}) %all-to-all-start.1) | async-done | bytes 1048608 | tf_op jit(solution)/shard_map/all_to_all | solution.py:15
  101.5 0.6 gather_fusion.3
  102.2 0.6 gather_fusion.2
  102.8 0.1 reshape.170
  102.9 9.2 %while.18 = (s32[]{:T(128)}, bf16[2,128,2,64]{1,3,2,0:T(8,128)(2,1)S(1)}, f32[2,8,32,2,64]{4,3,2,1,0:T(2,128)S(1)}, f32[2,8,32,2,64]{4,3,2,1,0:T(2,128)S(1)}, f3...) while((s32[]{:T(128)}, ...), condition=%wide.region_3.4_spmd, body=%wide.region_1.3_spmd.sunk | while | flops 76594944 | bytes 6599905 | solution.py:153
  103.1 0.2 fusion.157
  103.5 0.2 convolution_bitcast_fusion.7
  103.7 0.2 fusion.161
  104.0 0.2 fusion.162
  104.2 0.2 fusion.156
  104.5 0.2 fusion.166
  104.7 0.2 fusion.165
  104.8 0.5 copy_dynamic-update-slice_fusion.3
  105.3 0.2 convolution_bitcast_fusion.8
  105.5 0.2 fusion.163
  105.8 0.2 fusion.164
  105.9 0.1 convolution_multiply_fusion.3
  106.1 1.3 dynamic_update_slice.29
  107.4 0.1 fusion.167
  107.7 0.2 fusion.157
  108.1 0.2 convolution_bitcast_fusion.7
  108.3 0.2 fusion.161
  108.6 0.2 fusion.162
  108.8 0.2 fusion.156
  109.1 0.2 fusion.166
  109.3 0.2 fusion.165
  109.5 0.5 copy_dynamic-update-slice_fusion.3
  109.9 0.2 convolution_bitcast_fusion.8
  110.1 0.2 fusion.163
  110.4 0.2 fusion.164
  110.5 0.1 convolution_multiply_fusion.3
  110.7 1.3 dynamic_update_slice.29
  112.0 0.1 fusion.167
  112.1 0.5 stack_reshape.14
  112.6 0.5 stack_reshape.15
  113.1 2.6 %fusion.85 = (bf16[2,72,4096]{2,1,0:T(8,128)(2,1)S(1)}, f32[2,72,4096]{2,1,0:T(8,128)}) fusion(s32[16]{0:T(128)S(1)} %eq.46, pred[16]{0:T(512)(128)(4,1)S(1)} %and.45, f32[1,16,4096]{2,1,0:T(8,128)S(1)} %stack_reshape.15, f32[1,16,4096]{2,1,0:T(8,128)S(1)} %stack_reshape.14), kind=kOutput, calls=%fused_computation.144 | convolution fusion | flops 113969408 | bytes 4063312 | tf_op jit(solution)/shard_map/ab,xac->xbc/dot_general | solution.py:163
  116.0 1.1 pad_maximum_fusion.1
  117.1 6.0 %all-to-all-start.2 = ((bf16[64,2,32,128]{3,2,1,0:T(8,128)(2,1)}), bf16[64,2,32,128]{3,2,1,0:T(8,128)(2,1)S(1)}, u32[]{:S(2)}, u32[]{:S(2)}) async-start(bf16[64,2,32,128]{3,2,1,0:T(8,128)(2,1)} %pad_maximum_fusion.1), calls=%async_computation.2 | async-start | bytes 2097152 | tf_op jit(solution)/shard_map/all_to_all | solution.py:15
  123.2 0.2 copy.112
  123.3 0.3 reshape.181
  123.6 53.7 %all-to-all-done.2 = bf16[64,2,32,128]{3,2,1,0:T(8,128)(2,1)S(1)} async-done(((bf16[64,2,32,128]{3,2,1,0:T(8,128)(2,1)}), bf16[64,2,32,128]{3,2,1,0:T(8,128)(2,1)S(1)}, u32[]{:S(2)}, u32[]{:S(2)}) %all-to-all-start.2) | async-done | bytes 1048608 | tf_op jit(solution)/shard_map/all_to_all | solution.py:15
  177.3 1.1 broadcast_in_dim.114
  178.4 4.3 %all-to-all-start.3 = ((bf16[8,256,256]{1,2,0:T(8,128)(2,1)}), bf16[8,256,256]{1,2,0:T(8,128)(2,1)S(1)}, u32[]{:S(2)}, u32[]{:S(2)}) async-start(bf16[8,256,256]{1,2,0:T(8,128)(2,1)} %broadcast_in_dim.114), calls=%async_computation.3 | async-start | bytes 2097152 | tf_op jit(solution)/shard_map/all_to_all | solution.py:21
  182.8 0.2 stack_reshape.16
  183.0 0.2 stack_reshape.17
  183.2 1.2 fusion.60
  184.5 14.1 %all-to-all-done.3 = bf16[8,256,256]{1,2,0:T(8,128)(2,1)S(1)} async-done(((bf16[8,256,256]{1,2,0:T(8,128)(2,1)}), bf16[8,256,256]{1,2,0:T(8,128)(2,1)S(1)}, u32[]{:S(2)}, u32[]{:S(2)}) %all-to-all-start.3) | async-done | bytes 1048608 | tf_op jit(solution)/shard_map/all_to_all | solution.py:21
  198.6 0.5 fusion.61
  199.1 1.0 copy.114
  200.1 6.0 %all-to-all-start.4 = ((bf16[64,32,128]{2,1,0:T(8,128)(2,1)}), bf16[64,32,128]{2,1,0:T(8,128)(2,1)S(1)}, u32[]{:S(2)}, u32[]{:S(2)}) async-start(bf16[64,32,128]{2,1,0:T(8,128)(2,1)} %bitcast.53), calls=%async_computation.4 | async-start | bytes 1048576 | tf_op jit(solution)/shard_map/all_to_all | solution.py:45
  206.3 0.7 reshape.238
  207.2 0.7 copy.117
  208.1 0.7 copy.116
  208.9 29.6 %all-to-all-done.4 = bf16[64,32,128]{2,1,0:T(8,128)(2,1)S(1)} async-done(((bf16[64,32,128]{2,1,0:T(8,128)(2,1)}), bf16[64,32,128]{2,1,0:T(8,128)(2,1)S(1)}, u32[]{:S(2)}, u32[]{:S(2)}) %all-to-all-start.4) | async-done | bytes 524320 | tf_op jit(solution)/shard_map/all_to_all | solution.py:45
  238.5 0.7 convert_reduce_fusion
  (76 shorter events, 3.7 us)
Async XLA Ops:
  40.6 6.5 %copy-start.1 = (bf16[256,128]{1,0:T(8,128)(2,1)S(1)}, bf16[256,128]{1,0:T(8,128)(2,1)}, u32[]{:S(2)}) copy-start(bf16[256,128]{1,0:T(8,128)(2,1)} %param.11) | copy-start | bytes 196612
  40.7 6.6 %copy-start = (bf16[256,128]{1,0:T(8,128)(2,1)S(1)}, bf16[256,128]{1,0:T(8,128)(2,1)}, u32[]{:S(2)}) copy-start(bf16[256,128]{1,0:T(8,128)(2,1)} %param.10) | copy-start | bytes 196612
  40.7 7.1 %copy-start.3 = (bf16[256,128]{1,0:T(8,128)(2,1)S(1)}, bf16[256,128]{1,0:T(8,128)(2,1)}, u32[]{:S(2)}) copy-start(bf16[256,128]{1,0:T(8,128)(2,1)} %param.9) | copy-start | bytes 196612
  40.7 7.3 %copy-start.4 = (bf16[256,128]{1,0:T(8,128)(2,1)S(1)}, bf16[256,128]{1,0:T(8,128)(2,1)}, u32[]{:S(2)}) copy-start(bf16[256,128]{1,0:T(8,128)(2,1)} %param.13) | copy-start | bytes 196612
  41.8 59.5 %all-to-all-start.1 = ((bf16[64,2,32,128]{3,2,1,0:T(8,128)(2,1)}), bf16[64,2,32,128]{3,2,1,0:T(8,128)(2,1)S(1)}, u32[]{:S(2)}, u32[]{:S(2)}) async-start(bf16[64,2,32,128]{3,2,1,0:T(8,128)(2,1)} %pad_maximum_fusion), calls=%async_computation.1 | async-start | bytes 2097152 | tf_op jit(solution)/shard_map/all_to_all | solution.py:15
  101.3 1.6 copy-start.7
  112.1 3.6 %copy-start.5 = (bf16[2,128,2,64]{1,3,2,0:T(8,128)(2,1)}, bf16[2,128,2,64]{1,3,2,0:T(8,128)(2,1)S(1)}, u32[]{:S(2)}) copy-start(bf16[2,128,2,64]{1,3,2,0:T(8,128)(2,1)S(1)} %get-tuple-element.80) | copy-start | bytes 196612
  116.0 7.1 %copy-start.2 = (bf16[256,256]{1,0:T(8,128)(2,1)S(1)}, bf16[256,256]{1,0:T(8,128)(2,1)}, u32[]{:S(2)}) copy-start(bf16[256,256]{1,0:T(8,128)(2,1)} %param.15) | copy-start | bytes 393220
  117.1 60.2 %all-to-all-start.2 = ((bf16[64,2,32,128]{3,2,1,0:T(8,128)(2,1)}), bf16[64,2,32,128]{3,2,1,0:T(8,128)(2,1)S(1)}, u32[]{:S(2)}, u32[]{:S(2)}) async-start(bf16[64,2,32,128]{3,2,1,0:T(8,128)(2,1)} %pad_maximum_fusion.1), calls=%async_computation.2 | async-start | bytes 2097152 | tf_op jit(solution)/shard_map/all_to_all | solution.py:15
  178.4 20.2 %all-to-all-start.3 = ((bf16[8,256,256]{1,2,0:T(8,128)(2,1)}), bf16[8,256,256]{1,2,0:T(8,128)(2,1)S(1)}, u32[]{:S(2)}, u32[]{:S(2)}) async-start(bf16[8,256,256]{1,2,0:T(8,128)(2,1)} %broadcast_in_dim.114), calls=%async_computation.3 | async-start | bytes 2097152 | tf_op jit(solution)/shard_map/all_to_all | solution.py:21
  184.4 21.7 %copy-start.6 = (bf16[2,128,2,64]{1,3,2,0:T(8,128)(2,1)S(1)}, bf16[2,128,2,64]{1,3,2,0:T(8,128)(2,1)}, u32[]{:S(2)}) copy-start(bf16[2,128,2,64]{1,3,2,0:T(8,128)(2,1)} %copy-done.5) | copy-start | bytes 196612
  200.1 38.4 %all-to-all-start.4 = ((bf16[64,32,128]{2,1,0:T(8,128)(2,1)}), bf16[64,32,128]{2,1,0:T(8,128)(2,1)S(1)}, u32[]{:S(2)}, u32[]{:S(2)}) async-start(bf16[64,32,128]{2,1,0:T(8,128)(2,1)} %bitcast.53), calls=%async_computation.4 | async-start | bytes 1048576 | tf_op jit(solution)/shard_map/all_to_all | solution.py:45
where the time goes:
time: 240 us; the launch traced here: 239 us
  waiting for transfers between devices  150 us (62%)
  blocking collectives  32.3 us (13%)
  starting transfers between devices  21.6 us (9%)
  local copies, waits for them, and re-layouts  16.8 us (7%)
  matrix products  8.65 us (4%)
  other arithmetic  8.08 us (3%)
    all_to_all x2, waiting for transfers between devices, in_one_piece(): lax.all_to_all(both, axis, split_axis=split_dim, concat_axis=concat_dim,...  107 us
    all_to_all x1, blocking collectives, body(): lax.all_to_all(wanted.reshape(devices, groups), 'kv', split_axis=0, conca...  32.3 us
    all_to_all x1, waiting for transfers between devices, sum_at_owner(): lax.all_to_all(blocks, axis, split_axis=0, concat_axis=0, tiled=True)  29.6 us
    all_to_all x1, waiting for transfers between devices, from_everyone(): lax.all_to_all(jnp.broadcast_to(value[None], (count, *value.shape)), axis...  14.1 us
    all_to_all x2, starting transfers between devices, in_one_piece(): lax.all_to_all(both, axis, split_axis=split_dim, concat_axis=concat_dim,...  11.3 us
    all_to_all x1, starting transfers between devices, sum_at_owner(): lax.all_to_all(blocks, axis, split_axis=0, concat_axis=0, tiled=True)  5.96 us
  transfers between devices with their start and end apart: 4, of which 4 were waited for; matrix products, arithmetic and copies ran while one was open for 3% of the time, Pallas kernels for 0%

commit v1 on v0

v1 whole, which is shorter than its diff:
```python
import jax
import jax.numpy as jnp
from jax import lax
from jax.experimental import pallas as pl
from jax.experimental.pallas import tpu as pltpu
from jax.sharding import Mesh
from jax.sharding import PartitionSpec as P

KV = ("z", "y")
TP = ("x", "c")
QB = 128
KB = 32
HD = 64
SEL = 8
F32 = jnp.float32
BF16 = jnp.bfloat16


def iota(shape, dim):
    return lax.broadcasted_iota(jnp.int32, shape, dim)


def swap(x):
    return pltpu.roll(x, HD, 1)


def side_by_side(a, b):
    low = iota(a.shape, 1) < HD
    return jnp.where(low, a, swap(b)), jnp.where(low, swap(a), b)


def dot(a, b, dims=((1,), (0,))):
    return lax.dot_general(a, b, (dims, ((), ())), preferred_element_type=F32)


def pack_kernel(base_ref, chosen_ref, keys_ref, values_ref, out_ref):
    rows = keys_ref.shape[0]
    blocks = rows // KB
    packs = side_by_side(keys_ref[...].astype(F32), values_ref[...].astype(F32))
    lane = iota((1, 128), 1)
    high = jnp.zeros((1, 128), F32)
    low = jnp.zeros((1, 128), F32)
    for g in range(2):
        for s in range(SEL):
            entry = chosen_ref[g, s] + 1
            here = lane == base_ref[0] + (g * SEL + s)
            high = jnp.where(here, (entry >> 3).astype(F32), high)
            low = jnp.where(here, (entry & 7).astype(F32), low)
    shape = (KB * 16, rows)
    row, col = iota(shape, 0), iota(shape, 1)
    kind = row & 15
    perm = jnp.where((kind < blocks) & (col == kind * KB + (row >> 4)), 1.0, 0.0).astype(BF16)
    kind = iota((KB * 16, 128), 0) & 15
    extra = jnp.where(kind == 8, high, 0.0) + jnp.where(kind == 9, low, 0.0)
    for h in range(2):
        out_ref[h * KB * 16 : (h + 1) * KB * 16, :] = (dot(perm, packs[h].astype(BF16)) + extra).astype(BF16)


def select_kernel(got_ref, out_ref, ids_ref):
    got = got_ref[...].astype(F32).reshape(64, 2, 8, 128)
    table = got[:, 0].reshape(512, 128).astype(BF16)
    meta = got[:, 1].reshape(8, 8, 8, 128).sum(axis=1)
    ids = meta[:, 0] * 8.0 + meta[:, 1]
    ids_ref[...] = ids
    columns = ids.T
    number = (iota((128, 512), 1) + 1).astype(F32)
    for j in range(8):
        hot = jnp.where(number == columns[:, j : j + 1], 1.0, 0.0).astype(BF16)
        out_ref[j * 128 : (j + 1) * 128, :] = dot(hot, table).astype(BF16)


def attend_kernel(chosen_ref, queries_ref, keys_ref, values_ref, grad_ref, sums_ref, got_ref, dq_ref, back_ref, own_ref):
    lane = iota((QB, 128), 1)
    causal = iota((QB, QB), 0) <= iota((QB, QB), 1)
    sub = iota((SEL, QB), 0)
    for g in range(2):
        span = slice(g * QB, (g + 1) * QB)
        own_packs = side_by_side(keys_ref[span, :].astype(F32), values_ref[span, :].astype(F32))
        q = queries_ref[span, :].astype(F32) * (HD**-0.5)
        do = grad_ref[span, :].astype(F32)
        used = jnp.zeros((SEL, QB), jnp.int32)
        for s in range(SEL):
            used = jnp.where(sub == s, chosen_ref[g, s] + 1, used)
        used = (used > 0)[None]
        dq_parts = []
        for h in range(2):
            chosen_rows = got_ref[h * KB : (h + 1) * KB].astype(F32)[:, g * SEL : (g + 1) * SEL, :]
            pairs = jnp.concatenate([chosen_rows.reshape(KB * SEL, 128), own_packs[h]], axis=0).astype(BF16)
            q_low = jnp.where(lane < HD, q if h == 0 else swap(q), 0.0).astype(BF16)
            do_high = jnp.where(lane >= HD, do if h == 1 else swap(do), 0.0).astype(BF16)
            scores = dot(pairs, q_low, ((1,), (1,)))
            dots = dot(pairs, do_high, ((1,), (1,)))
            raw = jnp.exp(scores - sums_ref[h : h + 1, span])
            picked = jnp.where(used, raw[: KB * SEL].reshape(KB, SEL, QB), 0.0).reshape(KB * SEL, QB)
            weights = jnp.concatenate([picked, jnp.where(causal, raw[KB * SEL :], 0.0)], axis=0)
            low = weights.astype(BF16)
            deltas = jnp.sum(low.astype(F32) * dots, axis=0, keepdims=True)
            slopes = (weights * (dots - deltas)).astype(BF16)
            terms = dot(slopes, q_low) + dot(low, do_high)
            back_ref[h * KB : (h + 1) * KB, g * SEL : (g + 1) * SEL, :] = (
                terms[: KB * SEL].reshape(KB, SEL, 128).astype(BF16)
            )
            own_ref[h, span, :] = terms[KB * SEL :]
            dq_parts.append(dot(slopes, pairs, ((0,), (0,))) * (HD**-0.5))
        dq_ref[span, :] = jnp.where(lane < HD, dq_parts[0], swap(dq_parts[1])).astype(BF16)


def gather_kernel(ids_ref, got_ref, out_ref):
    number = (iota((512, 128), 0) + 1).astype(F32)
    total = jnp.zeros((512, 128), F32)
    for j in range(8):
        hot = jnp.where(number == ids_ref[j : j + 1, :], 1.0, 0.0).astype(BF16)
        total = total + dot(hot, got_ref[j * 128 : (j + 1) * 128, :])
    out_ref[...] = total.astype(BF16)


def finish_kernel(got_ref, own_ref, normed_ref, dk_ref, dv_ref, part_ref):
    rows = own_ref.shape[1]
    row, col = iota((rows, rows), 0), iota((rows, rows), 1)
    perm = jnp.where(col == (row & (KB - 1)) * 8 + (row >> 5), 1.0, 0.0).astype(BF16)
    first = dot(perm, got_ref[:rows, :]) + own_ref[0]
    second = dot(perm, got_ref[rows:, :]) + own_ref[1]
    low = iota((rows, 128), 1) < HD
    dk_ref[...] = jnp.where(low, first, swap(second)).astype(BF16)
    dv = jnp.where(low, swap(first), second).astype(BF16)
    dv_ref[...] = dv
    for t in range(8):
        part = dot(normed_ref[t], dv).astype(BF16)
        for zz in range(2):
            for y in range(4):
                k = zz * 4 + y
                part_ref[y, t * 2 + zz] = part[k * 32 : (k + 1) * 32, :]


VM = pl.BlockSpec(memory_space=pltpu.VMEM)
SM = pl.BlockSpec(memory_space=pltpu.SMEM)


def call(kernel, out, specs, name, *args):
    return pl.pallas_call(
        kernel,
        out_shape=out,
        in_specs=specs,
        out_specs=jax.tree.map(lambda _: VM, out),
        name=name,
    )(*args)


def shape(*dims, dtype=BF16):
    return jax.ShapeDtypeStruct(dims, dtype)


def exchange(x, axis):
    return lax.all_to_all(x, axis, split_axis=0, concat_axis=0, tiled=True)


def body(queries, keys, values, log_sums, out_grad, chosen, normed):
    rows = queries.shape[0]
    base = ((lax.axis_index(KV) % 8) * 16).astype(jnp.int32).reshape(1)
    with jax.named_scope("pieces"):
        pieces = call(pack_kernel, shape(1024, 128), [SM, SM, VM, VM], "pack", base, chosen, keys, values)
        pieces = exchange(pieces.reshape(64, 16, 128), KV)
    with jax.named_scope("features"):
        features = exchange(jnp.broadcast_to(normed.T[None], (8, *normed.shape)), TP)
    with jax.named_scope("picked"):
        picked, ids = call(
            select_kernel, (shape(1024, 128), shape(8, 128, dtype=F32)), [VM], "select", pieces.reshape(1024, 128)
        )
        picked = exchange(picked.reshape(64, 16, 128), KV)
    with jax.named_scope("attend"):
        query_grad, back, own = call(
            attend_kernel,
            (shape(rows, 128), shape(64, 16, 128), shape(2, rows, 128, dtype=F32)),
            [SM] + [VM] * 6,
            "attend",
            chosen, queries, keys, values, out_grad, log_sums, picked,
        )
    with jax.named_scope("back"):
        back = exchange(back, KV)
    with jax.named_scope("owner"):
        totals = call(gather_kernel, shape(512, 128), [VM, VM], "gather", ids, back.reshape(1024, 128))
        totals = exchange(totals.reshape(64, 8, 128), KV)
    with jax.named_scope("finish"):
        key_grad, value_grad, part = call(
            finish_kernel,
            (shape(rows, 128), shape(rows, 128), shape(4, 16, 32, 128)),
            [VM] * 3,
            "finish",
            totals.reshape(512, 128), own, features,
        )
    with jax.named_scope("sum_y"):
        part = exchange(part, "y").astype(F32).sum(axis=0).astype(BF16)
    with jax.named_scope("sum_z"):
        weight_grad = exchange(part, "z").astype(F32).sum(axis=0)
    return query_grad, key_grad, value_grad, weight_grad


def solution(mesh):
    fine = Mesh(mesh.devices.reshape(16, 4, 4, 2), ("z", "y", "x", "c"))
    both = P(KV, TP)
    in_specs = (both, both, both, P(TP, KV), both, P(KV, None), both)
    return jax.shard_map(body, mesh=fine, in_specs=in_specs, out_specs=(both,) * 4, check_vma=False)
```

time: 240 us -> 178 us (0.74)
  the two profiles are of different devices: /device:TPU:8 before, /device:TPU:32 now
where the time goes in v1:
time: 178 us
  blocking collectives  118 us (66%)
  waiting for transfers between devices  33.9 us (19%)
  Pallas kernels  12.5 us (7%)
  starting transfers between devices  10.2 us (6%)
    all_to_all x5, blocking collectives, exchange(): return lax.all_to_all(x, axis, split_axis=0, concat_axis=0, tiled=True)  118 us
    all_to_all x2, waiting for transfers between devices, exchange(): return lax.all_to_all(x, axis, split_axis=0, concat_axis=0, tiled=True)  33.9 us
    pallas_call x5, Pallas kernels, call(): pl.pallas_call(kernel, out_shape=out, in_specs=specs, out_specs=jax.tree....  12.5 us
    all_to_all x2, starting transfers between devices, exchange(): return lax.all_to_all(x, axis, split_axis=0, concat_axis=0, tiled=True)  10.2 us
  transfers between devices with their start and end apart: 2, of which 2 were waited for; matrix products, arithmetic and copies ran while one was open for 0% of the time, Pallas kernels for 1%

profile of v1, /device:TPU:32, one launch (start us, length us, event | category | flops | bytes accessed | tf_op | source)
XLA Modules:
  0.0 177.7 jit_solution(6159480078113858556)
XLA Ops:
  0.6 2.0 %pack.1 = bf16[1024,128]{1,0:T(8,128)(2,1)} custom-call(s32[1]{0:T(128)} %bitcast.base_ref, s32[2,8]{1,0:T(2,128)} %chosen_ref.3, bf16[256,128]{1,0:T(8,128)(2,1)} %keys_ref.3, bf16[256,128]{1,0:T(8,128)(2,1)} %values_ref.3), custom_call_target="tpu_custom_call" | custom-call | tf_op jit(solution)/shard_map/pieces/pack/pallas_call | solution.py:140
  2.6 40.3 %all_to_all.35 = bf16[64,16,128]{2,1,0:T(8,128)(2,1)} all-to-all(bf16[64,16,128]{2,1,0:T(8,128)(2,1)} %bitcast.10), channel_id=1, replica_groups=mesh['z'=16,'y'=4,'x'=4,'c'=2] {'z','y'}, dimensions={0} | all-to-all | bytes 524288 | tf_op jit(solution)/shard_map/pieces/all_to_all | solution.py:154
  43.0 2.2 %select.3 = (bf16[1024,128]{1,0:T(8,128)(2,1)}, f32[8,128]{1,0:T(8,128)}) custom-call(bf16[1024,128]{1,0:T(8,128)(2,1)} %bitcast.9), custom_call_target="tpu_custom_call" | custom-call | tf_op jit(solution)/shard_map/picked/select/pallas_call | solution.py:140
  45.2 26.4 %all_to_all.36.got_ref = bf16[64,16,128]{2,1,0:T(8,128)(2,1)} all-to-all(bf16[64,16,128]{2,1,0:T(8,128)(2,1)} %bitcast.13), channel_id=1, replica_groups=mesh['z'=16,'y'=4,'x'=4,'c'=2] {'z','y'}, dimensions={0} | all-to-all | bytes 524288 | tf_op jit(solution)/shard_map/picked/all_to_all | solution.py:154
  71.6 3.4 %attend.1 = (bf16[256,128]{1,0:T(8,128)(2,1)}, bf16[64,16,128]{2,1,0:T(8,128)(2,1)}, f32[2,256,128]{2,1,0:T(8,128)}) custom-call(s32[2,8]{1,0:T(2,128)} %chosen_ref.3, bf16[256,128]{1,0:T(8,128)(2,1)} %queries_ref.1, bf16[256,128]{1,0:T(8,128)(2,1)} %keys_ref.3, bf16[256,128]{1,0:T(8,128)(2,1)} %values_ref.3, bf16[256,128]{1,0:T(8,128)(2,1)} %grad_ref.1, ...), custom_call_target="tpu_custom_call" | custom-call | tf_op jit(solution)/shard_map/attend/attend/pallas_call | solution.py:140
  75.0 0.0 copy-start.2
  75.0 5.9 %all-to-all-start.2 = ((bf16[64,16,128]{2,1,0:T(8,128)(2,1)}), bf16[64,16,128]{2,1,0:T(8,128)(2,1)S(1)}, u32[]{:S(2)}, u32[]{:S(2)}) async-start(bf16[64,16,128]{2,1,0:T(8,128)(2,1)} %get-tuple-element.15), calls=%async_computation.2 | async-start | bytes 524288 | tf_op jit(solution)/shard_map/back/all_to_all | solution.py:154
  80.9 0.0 copy-done.2
  80.9 0.1 copy.12
  81.0 20.0 %all-to-all-done.2 = bf16[64,16,128]{2,1,0:T(8,128)(2,1)S(1)} async-done(((bf16[64,16,128]{2,1,0:T(8,128)(2,1)}), bf16[64,16,128]{2,1,0:T(8,128)(2,1)S(1)}, u32[]{:S(2)}, u32[]{:S(2)}) %all-to-all-start.2) | async-done | bytes 262176 | tf_op jit(solution)/shard_map/back/all_to_all | solution.py:154
  101.0 0.0 copy-start.1
  101.0 1.1 broadcast_in_dim.2
  102.1 0.0 copy-done.1
  102.1 4.3 %all-to-all-start.4 = ((bf16[8,256,256]{2,1,0:T(8,128)(2,1)}), bf16[8,256,256]{2,1,0:T(8,128)(2,1)S(1)}, u32[]{:S(2)}, u32[]{:S(2)}) async-start(bf16[8,256,256]{2,1,0:T(8,128)(2,1)} %broadcast_in_dim.2), calls=%async_computation.4 | async-start | bytes 2097152 | tf_op jit(solution)/shard_map/features/all_to_all | solution.py:154
  106.4 2.0 %gather.1 = bf16[512,128]{1,0:T(8,128)(2,1)} custom-call(f32[8,128]{1,0:T(8,128)} %get-tuple-element.14.ids_ref, bf16[1024,128]{1,0:T(8,128)(2,1)} %bitcast.8), custom_call_target="tpu_custom_call" | custom-call | tf_op jit(solution)/shard_map/owner/gather/pallas_call | solution.py:140
  108.5 13.9 %all-to-all-done.4.normed_ref = bf16[8,256,256]{2,1,0:T(8,128)(2,1)S(1)} async-done(((bf16[8,256,256]{2,1,0:T(8,128)(2,1)}), bf16[8,256,256]{2,1,0:T(8,128)(2,1)S(1)}, u32[]{:S(2)}, u32[]{:S(2)}) %all-to-all-start.4) | async-done | bytes 1048608 | tf_op jit(solution)/shard_map/features/all_to_all | solution.py:154
  122.4 0.0 copy-start
  122.4 23.3 %all_to_all.37 = bf16[64,8,128]{2,1,0:T(8,128)(2,1)} all-to-all(bf16[64,8,128]{2,1,0:T(8,128)(2,1)} %bitcast.11), channel_id=1, replica_groups=mesh['z'=16,'y'=4,'x'=4,'c'=2] {'z','y'}, dimensions={0} | all-to-all | bytes 262144 | tf_op jit(solution)/shard_map/owner/all_to_all | solution.py:154
  145.6 0.0 copy-done
  145.6 2.9 %finish.1 = (bf16[256,128]{1,0:T(8,128)(2,1)}, bf16[256,128]{1,0:T(8,128)(2,1)}, bf16[4,16,32,128]{3,2,1,0:T(8,128)(2,1)}) custom-call(bf16[512,128]{1,0:T(8,128)(2,1)} %bitcast.12, f32[2,256,128]{2,1,0:T(8,128)} %get-tuple-element.16.own_ref, bf16[8,256,256]{2,1,0:T(8,128)(2,1)} %copy-done), custom_call_target="tpu_custom_call" | custom-call | tf_op jit(solution)/shard_map/finish/finish/pallas_call | solution.py:140
  148.5 11.5 %all_to_all.38 = bf16[4,16,32,128]{3,2,1,0:T(8,128)(2,1)S(1)} all-to-all(bf16[4,16,32,128]{3,2,1,0:T(8,128)(2,1)} %get-tuple-element.19), channel_id=1, replica_groups=mesh['z'=16,'y'=4,'x'=4,'c'=2] {'y'}, dimensions={0} | all-to-all | bytes 1048576 | tf_op jit(solution)/shard_map/sum_y/all_to_all | solution.py:154
  160.0 0.1 reduce_sum.21
  160.1 17.0 %all_to_all.39 = bf16[16,32,128]{2,1,0:T(8,128)(2,1)S(1)} all-to-all(bf16[16,32,128]{2,1,0:T(8,128)(2,1)S(1)} %reduce_sum.21), channel_id=1, replica_groups=mesh['z'=16,'y'=4,'x'=4,'c'=2] {'z'}, dimensions={0} | all-to-all | bytes 262144 | tf_op jit(solution)/shard_map/sum_z/all_to_all | solution.py:154
  177.1 0.6 convert_reduce_fusion
Async XLA Ops:
  75.0 5.9 %copy-start.2 = (bf16[256,256]{1,0:T(8,128)(2,1)S(1)}, bf16[256,256]{1,0:T(8,128)(2,1)}, u32[]{:S(2)}) copy-start(bf16[256,256]{1,0:T(8,128)(2,1)} %param.13) | copy-start | bytes 393220
  75.0 26.1 %all-to-all-start.2 = ((bf16[64,16,128]{2,1,0:T(8,128)(2,1)}), bf16[64,16,128]{2,1,0:T(8,128)(2,1)S(1)}, u32[]{:S(2)}, u32[]{:S(2)}) async-start(bf16[64,16,128]{2,1,0:T(8,128)(2,1)} %get-tuple-element.15), calls=%async_computation.2 | async-start | bytes 524288 | tf_op jit(solution)/shard_map/back/all_to_all | solution.py:154
  101.0 1.1 copy-start.1
  102.1 20.2 %all-to-all-start.4 = ((bf16[8,256,256]{2,1,0:T(8,128)(2,1)}), bf16[8,256,256]{2,1,0:T(8,128)(2,1)S(1)}, u32[]{:S(2)}, u32[]{:S(2)}) async-start(bf16[8,256,256]{2,1,0:T(8,128)(2,1)} %broadcast_in_dim.2), calls=%async_computation.4 | async-start | bytes 2097152 | tf_op jit(solution)/shard_map/features/all_to_all | solution.py:154
  122.4 23.3 %copy-start = (bf16[8,256,256]{2,1,0:T(8,128)(2,1)}, bf16[8,256,256]{2,1,0:T(8,128)(2,1)S(1)}, u32[]{:S(2)}) copy-start(bf16[8,256,256]{2,1,0:T(8,128)(2,1)S(1)} %all-to-all-done.4.normed_ref) | copy-start | bytes 3145732

commit v2 on v1

v2 whole, which is shorter than its diff:
```python
import jax
import jax.numpy as jnp
from jax import lax
from jax.experimental import pallas as pl
from jax.experimental.pallas import tpu as pltpu
from jax.sharding import Mesh
from jax.sharding import PartitionSpec as P


KV = ("z", "y")
QB = 128
KB = 32
HD = 64
SEL = 8
F32 = jnp.float32
BF16 = jnp.bfloat16


def iota(shape, dim):
    return lax.broadcasted_iota(jnp.int32, shape, dim)


def dot(a, b, dims=((1,), (0,))):
    return lax.dot_general(a, b, (dims, ((), ())), preferred_element_type=F32)


def one_hot(hits):
    return jnp.where(hits, 1.0, 0.0).astype(BF16)


def pack_kernel(base_ref, chosen_ref, keys_ref, values_ref, out_ref):
    lane = iota((1, 128), 1)
    high = jnp.zeros((1, 128), F32)
    low = jnp.zeros((1, 128), F32)
    for g in range(2):
        for s in range(SEL):
            entry = chosen_ref[g, s] + 1
            here = lane == base_ref[0] + (g * SEL + s)
            high = jnp.where(here, (entry >> 3).astype(F32), high)
            low = jnp.where(here, (entry & 7).astype(F32), low)
    row, col = iota((KB * 16, 256), 0), iota((KB * 16, 256), 1)
    kind = row & 15
    perm = one_hot((kind < 8) & (col == kind * KB + (row >> 4)))
    kind = iota((KB * 16, 128), 0) & 15
    extra = jnp.where(kind == 8, high, 0.0) + jnp.where(kind == 9, low, 0.0)
    out_ref[: KB * 16, :] = (dot(perm, keys_ref[...]) + extra).astype(BF16)
    out_ref[KB * 16 :, :] = (dot(perm, values_ref[...]) + extra).astype(BF16)


def select_kernel(got_ref, out_ref, ids_ref):
    got = got_ref[...].astype(F32).reshape(64, 2, 8, 128)
    table = got[:, 0].reshape(512, 128).astype(BF16)
    meta = got[:, 1].reshape(8, 8, 8, 128).sum(axis=1)
    ids = meta[:, 0] * 8.0 + meta[:, 1]
    ids_ref[...] = ids
    columns = ids.T
    number = (iota((128, 512), 1) + 1).astype(F32)
    for j in range(8):
        hot = one_hot(number == columns[:, j : j + 1])
        out_ref[j * 128 : (j + 1) * 128, :] = dot(hot, table).astype(BF16)


def by_rest():
    row, col = iota((256, 256), 0), iota((256, 256), 1)
    return one_hot(col == (row & 7) * KB + ((row >> 3) & 7) * 4 + (row >> 6))


def attend_kernel(
    place_ref, chosen_ref, queries_ref, keys_ref, values_ref, grad_ref, sums_ref, got_ref, dq_ref, back_ref, own_ref
):
    lane = iota((QB, 128), 1)
    causal = iota((QB, QB), 0) <= iota((QB, QB), 1)
    sub = iota((SEL, QB), 0)
    own_k, own_v = [], []
    for g in range(2):
        span = slice(g * QB, (g + 1) * QB)
        got = got_ref[...].astype(F32)[:, g * SEL : (g + 1) * SEL, :].reshape(2, KB * SEL, 128).astype(BF16)
        keys = jnp.concatenate([got[0], keys_ref[span, :]], axis=0)
        values = jnp.concatenate([got[1], values_ref[span, :]], axis=0)
        q = queries_ref[span, :].astype(F32) * (HD**-0.5)
        do = grad_ref[span, :].astype(F32)
        used = jnp.zeros((SEL, QB), jnp.int32)
        for s in range(SEL):
            used = jnp.where(sub == s, chosen_ref[g, s] + 1, used)
        used = (used > 0)[None]
        dq_parts, dk, dv = [], 0.0, 0.0
        for h in range(2):
            mine = (lane >= HD) == (h == 1)
            q_h = jnp.where(mine, q, 0.0).astype(BF16)
            do_h = jnp.where(mine, do, 0.0).astype(BF16)
            scores = dot(keys, q_h, ((1,), (1,)))
            dots = dot(values, do_h, ((1,), (1,)))
            raw = jnp.exp(scores - sums_ref[h : h + 1, span])
            picked = jnp.where(used, raw[: KB * SEL].reshape(KB, SEL, QB), 0.0).reshape(KB * SEL, QB)
            weights = jnp.concatenate([picked, jnp.where(causal, raw[KB * SEL :], 0.0)], axis=0)
            low = weights.astype(BF16)
            deltas = jnp.sum(low.astype(F32) * dots, axis=0, keepdims=True)
            slopes = (weights * (dots - deltas)).astype(BF16)
            dk = dk + dot(slopes, q_h)
            dv = dv + dot(low, do_h)
            dq_parts.append(dot(slopes, keys, ((0,), (0,))))
        back_ref[:KB, g * SEL : (g + 1) * SEL, :] = dk[: KB * SEL].reshape(KB, SEL, 128).astype(BF16)
        back_ref[KB:, g * SEL : (g + 1) * SEL, :] = dv[: KB * SEL].reshape(KB, SEL, 128).astype(BF16)
        own_k.append(dk[KB * SEL :])
        own_v.append(dv[KB * SEL :])
        dq_ref[span, :] = (jnp.where(lane < HD, dq_parts[0], dq_parts[1]) * (HD**-0.5)).astype(BF16)
    perm = by_rest()
    for n, own in enumerate((own_k, own_v)):
        own = dot(perm, jnp.concatenate(own, axis=0).astype(BF16)).astype(BF16)
        for y in range(4):
            own_ref[(y - place_ref[0]) & 3, n] = own[y * 64 : (y + 1) * 64]


def gather_kernel(ids_ref, got_ref, out_ref):
    number = (iota((512, 128), 0) + 1).astype(F32)
    total = jnp.zeros((512, 128), F32)
    for j in range(8):
        hot = one_hot(number == ids_ref[j : j + 1, :])
        total = total + dot(hot, got_ref[j * 128 : (j + 1) * 128, :])
    out_ref[...] = total.astype(BF16)


def add_kernel(place_ref, got_ref, o0_ref, o1_ref, o2_ref, o3_ref, out_ref, acc_ref):
    acc_ref[...] = got_ref[...].astype(F32).reshape(2, 8, 4, 8, 128)
    for s, o_ref in enumerate((o0_ref, o1_ref, o2_ref, o3_ref)):
        y = (place_ref[0] - s) & 3
        acc_ref[:, :, y] = acc_ref[:, :, y] + o_ref[...].astype(F32).reshape(2, 8, 8, 128)
    values = acc_ref[1].reshape(256, 128).astype(BF16)
    for y in range(4):
        out_ref[y, :256, :] = values
        out_ref[y, 256:, :] = acc_ref[0, :, y].reshape(64, 128).astype(BF16)


def turn_kernel(place_ref, normed_ref, out_ref):
    turned = dot(normed_ref[...], by_rest(), ((0,), (1,))).astype(BF16).reshape(2, 4, 32, 256)
    for y in range(4):
        for zz in range(2):
            out_ref[(y - place_ref[0]) & 3, zz * 32 : (zz + 1) * 32, :] = turned[zz, y]


def finish_kernel(place_ref, got_ref, f0_ref, f1_ref, f2_ref, f3_ref, dk_ref, dv_ref, part_ref, acc_ref):
    got = got_ref[...].astype(F32)
    acc_ref[...] = got[:, :256].reshape(4, 8, 4, 8, 128)
    total = 0.0
    for s in range(4):
        value = acc_ref[:, :, (place_ref[0] - s) & 3].reshape(256, 128).astype(BF16)
        rows = [f_ref[c, s] for f_ref in (f0_ref, f1_ref, f2_ref, f3_ref) for c in range(2)]
        total = total + dot(jnp.concatenate(rows, axis=0), value)
        if s == 0:
            mine = value
    total = total.astype(BF16)
    for s in range(4):
        for c in range(2):
            t = ((place_ref[1] - s) & 3) * 2 + ((place_ref[2] + c) & 1)
            k = (s * 2 + c) * 64
            part_ref[t] = total[k : k + 64]
    perm = by_rest()
    dv_ref[...] = dot(perm, mine, ((0,), (0,))).astype(BF16)
    dk_ref[...] = dot(perm, got[:, 256:].reshape(256, 128).astype(BF16), ((0,), (0,))).astype(BF16)


VM = pl.BlockSpec(memory_space=pltpu.VMEM)
SM = pl.BlockSpec(memory_space=pltpu.SMEM)


def call(kernel, out, specs, *args, scratch=()):
    args = [pltpu.with_memory_space_constraint(a, pltpu.VMEM) if s is VM else a for a, s in zip(args, specs)]
    return pl.pallas_call(
        kernel,
        out_shape=jax.tree.map(lambda o: pltpu.VMEM(o.shape, o.dtype), out),
        in_specs=specs,
        out_specs=jax.tree.map(lambda _: VM, out),
        scratch_shapes=scratch,
    )(*args)


def shape(*dims, dtype=BF16):
    return jax.ShapeDtypeStruct(dims, dtype)


def exchange(x, axis):
    return lax.all_to_all(x, axis, split_axis=0, concat_axis=0, tiled=True)


def shift(x, axis, by):
    size = lax.axis_size(axis)
    return lax.ppermute(x, axis, [(n, (n + by) % size) for n in range(size)])


def body(queries, keys, values, log_sums, out_grad, chosen, normed):
    rows = queries.shape[0]
    base = ((lax.axis_index("z") * 4 + lax.axis_index("y")) & 7) * 16
    base = base.astype(jnp.int32).reshape(1)
    place = jnp.stack([lax.axis_index("y"), lax.axis_index("x"), lax.axis_index("c")]).astype(jnp.int32)
    pieces = call(pack_kernel, shape(1024, 128), [SM, SM, VM, VM], base, chosen, keys, values)
    pieces = exchange(pieces.reshape(64, 16, 128), KV)
    turned = call(turn_kernel, shape(4, 64, 256), [SM, VM], place, normed)
    features = jnp.stack([turned[0]] + [shift(turned[s], "y", s) for s in range(1, 4)])
    features = jnp.stack([features, shift(features, "c", 1)])
    features = [features] + [shift(features, "x", s) for s in range(1, 4)]
    picked, ids = call(
        select_kernel, (shape(1024, 128), shape(8, 128, dtype=F32)), [VM], pieces.reshape(1024, 128)
    )
    picked = exchange(picked.reshape(64, 16, 128), KV)
    query_grad, back, own = call(
        attend_kernel,
        (shape(rows, 128), shape(64, 16, 128), shape(4, 2, 64, 128)),
        [SM, SM] + [VM] * 6,
        place, chosen, queries, keys, values, out_grad, log_sums, picked,
    )
    own = [own[0]] + [shift(own[s], "y", s) for s in range(1, 4)]
    back = exchange(back, KV)
    sums = call(gather_kernel, shape(512, 128), [VM, VM], ids, back.reshape(1024, 128))
    sums = exchange(sums.reshape(16, 32, 128), "z")
    sums = call(
        add_kernel,
        shape(4, 320, 128),
        [SM] + [VM] * 5,
        place, sums, *own,
        scratch=[pltpu.VMEM((2, 8, 4, 8, 128), F32)],
    )
    sums = exchange(sums, "y")
    key_grad, value_grad, part = call(
        finish_kernel,
        (shape(rows, 128), shape(rows, 128), shape(8, 64, 128)),
        [SM] + [VM] * 5,
        place, sums, *features,
        scratch=[pltpu.VMEM((4, 8, 4, 8, 128), F32)],
    )
    weight_grad = exchange(part.reshape(16, 32, 128), "z").astype(F32).sum(axis=0)
    return query_grad, key_grad, value_grad, weight_grad


def solution(mesh):
    fine = Mesh(mesh.devices.reshape(16, 4, 4, 2), ("z", "y", "x", "c"))
    both = P(KV, ("x", "c"))
    in_specs = (both, both, both, P(("x", "c"), KV), both, P(KV, None), both)
    return jax.shard_map(body, mesh=fine, in_specs=in_specs, out_specs=(both,) * 4, check_vma=False)
```

time: 178 us -> 170 us (0.955)
  the two profiles are of different devices: /device:TPU:32 before, /device:TPU:2 now
where the time goes in v2:
time: 170 us; the launch traced here: 169 us
  starting transfers between devices  61.3 us (36%)
  waiting for transfers between devices  50.1 us (29%)
  blocking collectives  41 us (24%)
  Pallas kernels  10.5 us (6%)
  local copies, waits for them, and re-layouts  3.61 us (2%)
    all_to_all x5, waiting for transfers between devices, exchange(): return lax.all_to_all(x, axis, split_axis=0, concat_axis=0, tiled=True)  47.4 us
    all_to_all x1, blocking collectives, exchange(): return lax.all_to_all(x, axis, split_axis=0, concat_axis=0, tiled=True)  41 us
    ppermute x10, starting transfers between devices, shift(): return lax.ppermute(x, axis, [(n, (n + by) % size) for n in range(size)])  31.7 us
    all_to_all x5, starting transfers between devices, exchange(): return lax.all_to_all(x, axis, split_axis=0, concat_axis=0, tiled=True)  29.6 us
    pallas_call x7, Pallas kernels, call(): pl.pallas_call(kernel, out_shape=jax.tree.map(lambda o: pltpu.VMEM(o.shap...  10.5 us
    unnamed x19, local copies, waits for them, and re-layouts  3.59 us
  transfers between devices with their start and end apart: 15, of which 6 were waited for; matrix products, arithmetic and copies ran while one was open for 2% of the time, Pallas kernels for 2%

profile of v2, /device:TPU:2, one launch (start us, length us, event | category | flops | bytes accessed | tf_op | source)
XLA Modules:
  0.0 168.7 jit_solution(2772649008046105059)
XLA Ops:
  0.6 0.0 copy-start
  0.7 0.8 copy-done
  1.5 0.0 copy-start.2
  1.5 0.8 copy-done.2
  2.3 1.0 shard_map.102
  3.3 41.0 %all_to_all.30 = bf16[64,16,128]{2,1,0:T(8,128)(2,1)S(1)} all-to-all(bf16[64,16,128]{2,1,0:T(8,128)(2,1)S(1)} %bitcast.32), channel_id=1, replica_groups=mesh['z'=16,'y'=4,'x'=4,'c'=2] {'z','y'}, dimensions={0} | all-to-all | bytes 524288 | tf_op jit(solution)/shard_map/all_to_all | solution.py:182
  44.3 1.3 shard_map.103
  45.6 0.0 copy-start.1
  45.6 0.0 copy-start.3
  45.6 0.0 copy-start.5
  45.6 0.0 copy-start.6
  45.6 5.1 %all-to-all-start.1 = ((bf16[64,16,128]{2,1,0:T(8,128)(2,1)}), bf16[64,16,128]{2,1,0:T(8,128)(2,1)S(1)}, u32[]{:S(2)}, u32[]{:S(2)}) async-start(bf16[64,16,128]{2,1,0:T(8,128)(2,1)} %bitcast.6), calls=%async_computation.1 | async-start | bytes 524288 | tf_op jit(solution)/shard_map/all_to_all | solution.py:182
  50.7 0.0 copy-start.7
  50.8 0.6 pad_add_fusion.place_ref
  51.3 21.2 %all-to-all-done.1.got_ref = bf16[64,16,128]{2,1,0:T(8,128)(2,1)S(1)} async-done(((bf16[64,16,128]{2,1,0:T(8,128)(2,1)}), bf16[64,16,128]{2,1,0:T(8,128)(2,1)S(1)}, u32[]{:S(2)}, u32[]{:S(2)}) %all-to-all-start.1) | async-done | bytes 262176 | tf_op jit(solution)/shard_map/all_to_all | solution.py:182
  72.5 0.0 copy-done.1
  72.5 0.0 copy-done.3
  72.5 0.0 copy-done.5
  72.5 0.0 copy-done.6
  72.5 0.0 copy-done.7
  72.5 2.9 %shard_map.104 = (bf16[256,128]{1,0:T(8,128)(2,1)S(1)}, bf16[64,16,128]{2,1,0:T(8,128)(2,1)}, bf16[4,2,64,128]{3,2,1,0:T(8,128)(2,1)S(1)}) custom-call(s32[3]{0:T(128)} %pad_add_fusion.place_ref, s32[2,8]{1,0:T(2,128)} %chosen_ref.3, bf16[256,128]{1,0:T(8,128)(2,1)S(1)} %copy-done.5, bf16[256,128]{1,0:T(8,128)(2,1)S(1)} %copy-done.1, ...), custom_call_target="tpu_custom_call" | custom-call | tf_op jit(solution)/shard_map/pallas_call | solution.py:168
  75.4 0.0 copy-start.4
  75.4 4.8 %all-to-all-start.2 = ((bf16[64,16,128]{2,1,0:T(8,128)(2,1)}), bf16[64,16,128]{2,1,0:T(8,128)(2,1)S(1)}, u32[]{:S(2)}, u32[]{:S(2)}) async-start(bf16[64,16,128]{2,1,0:T(8,128)(2,1)} %get-tuple-element.15), calls=%async_computation.2 | async-start | bytes 524288 | tf_op jit(solution)/shard_map/all_to_all | solution.py:182
  80.2 0.0 copy-done.4
  80.2 0.9 shard_map.107
  81.2 4.7 %collective-permute-start.5 = (bf16[64,256]{1,0:T(8,128)(2,1)S(1)}, bf16[64,256]{1,0:T(8,128)(2,1)S(1)}, u32[]{:S(2)}, u32[]{:S(2)}) collective-permute-start(bf16[64,256]{1,0:T(8,128)(2,1)S(1)} %get-tuple-element.23), channel_id=1, source_target_pairs={{0,24},{8,0},{16,8},{24,16},{1,25},{9,1},{17,9},{25,17},{2,26},{10... | collective-permute-start | bytes 98312 | tf_op jit(solution)/shard_map/ppermute | solution.py:187
  85.9 2.8 %collective-permute-start.4 = (bf16[64,256]{1,0:T(8,128)(2,1)S(1)}, bf16[64,256]{1,0:T(8,128)(2,1)S(1)}, u32[]{:S(2)}, u32[]{:S(2)}) collective-permute-start(bf16[64,256]{1,0:T(8,128)(2,1)S(1)} %get-tuple-element.24), channel_id=1, source_target_pairs={{0,16},{8,24},{16,0},{24,8},{1,17},{9,25},{17,1},{25,9},{2,18},{10... | collective-permute-start | bytes 98312 | tf_op jit(solution)/shard_map/ppermute | solution.py:187
  88.6 2.8 %collective-permute-start.3 = (bf16[64,256]{1,0:T(8,128)(2,1)S(1)}, bf16[64,256]{1,0:T(8,128)(2,1)S(1)}, u32[]{:S(2)}, u32[]{:S(2)}) collective-permute-start(bf16[64,256]{1,0:T(8,128)(2,1)S(1)} %get-tuple-element.25), channel_id=1, source_target_pairs={{0,8},{8,16},{16,24},{24,0},{1,9},{9,17},{17,25},{25,1},{2,10},{10... | collective-permute-start | bytes 98312 | tf_op jit(solution)/shard_map/ppermute | solution.py:187
  91.4 10.6 %all-to-all-done.2 = bf16[64,16,128]{2,1,0:T(8,128)(2,1)S(1)} async-done(((bf16[64,16,128]{2,1,0:T(8,128)(2,1)}), bf16[64,16,128]{2,1,0:T(8,128)(2,1)S(1)}, u32[]{:S(2)}, u32[]{:S(2)}) %all-to-all-start.2) | async-done | bytes 262176 | tf_op jit(solution)/shard_map/all_to_all | solution.py:182
  102.1 1.1 shard_map.105
  103.1 3.5 %all-to-all-start.3 = ((bf16[16,32,128]{2,1,0:T(8,128)(2,1)}), bf16[16,32,128]{2,1,0:T(8,128)(2,1)S(1)}, u32[]{:S(2)}, u32[]{:S(2)}) async-start(bf16[16,32,128]{2,1,0:T(8,128)(2,1)} %bitcast.8), calls=%async_computation.3 | async-start | bytes 262144 | tf_op jit(solution)/shard_map/all_to_all | solution.py:182
  106.6 0.0 collective-permute-done.5
  106.7 0.0 collective-permute-done.4
  106.7 0.0 collective-permute-done.3
  106.7 1.9 %collective-permute-start.6 = (bf16[4,64,256]{2,1,0:T(8,128)(2,1)S(1)}, bf16[4,64,256]{2,1,0:T(8,128)(2,1)S(1)}, u32[]{:S(2)}, u32[]{:S(2)}) collective-permute-start(bf16[4,64,256]{2,1,0:T(8,128)(2,1)S(1)} %get-tuple-element.21), channel_id=1, source_target_pairs={{0,1},{1,0},{2,3},{3,2},{4,5},{5,4},{6,7},{7,6},{8,9},{9,8},{10,11... | collective-permute-start | bytes 393224 | tf_op jit(solution)/shard_map/ppermute | solution.py:187
  108.7 3.5 %collective-permute-start.2 = (bf16[2,64,128]{2,1,0:T(8,128)(2,1)S(1)}, bf16[2,64,128]{2,1,0:T(8,128)(2,1)S(1)}, u32[]{:S(2)}, u32[]{:S(2)}) collective-permute-start(bf16[2,64,128]{2,1,0:T(8,128)(2,1)S(1)} %get-tuple-element.26), channel_id=1, source_target_pairs={{0,24},{8,0},{16,8},{24,16},{1,25},{9,1},{17,9},{25,17},{2,26},{10... | collective-permute-start | bytes 98312 | tf_op jit(solution)/shard_map/ppermute | solution.py:187
  112.1 3.2 %collective-permute-start.1 = (bf16[2,64,128]{2,1,0:T(8,128)(2,1)S(1)}, bf16[2,64,128]{2,1,0:T(8,128)(2,1)S(1)}, u32[]{:S(2)}, u32[]{:S(2)}) collective-permute-start(bf16[2,64,128]{2,1,0:T(8,128)(2,1)S(1)} %get-tuple-element.27), channel_id=1, source_target_pairs={{0,16},{8,24},{16,0},{24,8},{1,17},{9,25},{17,1},{25,9},{2,18},{10... | collective-permute-start | bytes 98312 | tf_op jit(solution)/shard_map/ppermute | solution.py:187
  115.3 2.3 %collective-permute-start = (bf16[2,64,128]{2,1,0:T(8,128)(2,1)S(1)}, bf16[2,64,128]{2,1,0:T(8,128)(2,1)S(1)}, u32[]{:S(2)}, u32[]{:S(2)}) collective-permute-start(bf16[2,64,128]{2,1,0:T(8,128)(2,1)S(1)} %get-tuple-element.28), channel_id=1, source_target_pairs={{0,8},{8,16},{16,24},{24,0},{1,9},{9,17},{17,25},{25,1},{2,10},{10... | collective-permute-start | bytes 98312 | tf_op jit(solution)/shard_map/ppermute | solution.py:187
  117.6 0.0 collective-permute-done.6
  117.7 2.5 %collective-permute-start.9 = (bf16[2,4,64,256]{3,2,1,0:T(8,128)(2,1)S(1)}, bf16[2,4,64,256]{3,2,1,0:T(8,128)(2,1)S(1)}, u32[]{:S(2)}, u32[]{:S(2)}) collective-permute-start(bf16[2,4,64,256]{3,2,1,0:T(8,128)(2,1)S(1)} %pad_maximum_fusion.f0_ref), channel_id=1, source_target_pairs={{0,6},{2,0},{4,2},{6,4},{1,7},{3,1},{5,3},{7,5},{8,14},{10,8},{12,... | collective-permute-start | bytes 786440 | tf_op jit(solution)/shard_map/ppermute | solution.py:187
  120.2 4.3 %collective-permute-start.8 = (bf16[2,4,64,256]{3,2,1,0:T(8,128)(2,1)S(1)}, bf16[2,4,64,256]{3,2,1,0:T(8,128)(2,1)S(1)}, u32[]{:S(2)}, u32[]{:S(2)}) collective-permute-start(bf16[2,4,64,256]{3,2,1,0:T(8,128)(2,1)S(1)} %pad_maximum_fusion.f0_ref), channel_id=1, source_target_pairs={{0,4},{2,6},{4,0},{6,2},{1,5},{3,7},{5,1},{7,3},{8,12},{10,14},{12... | collective-permute-start | bytes 786440 | tf_op jit(solution)/shard_map/ppermute | solution.py:187
  124.6 0.0 collective-permute-done.2.o3_ref
  124.6 3.7 %collective-permute-start.7 = (bf16[2,4,64,256]{3,2,1,0:T(8,128)(2,1)S(1)}, bf16[2,4,64,256]{3,2,1,0:T(8,128)(2,1)S(1)}, u32[]{:S(2)}, u32[]{:S(2)}) collective-permute-start(bf16[2,4,64,256]{3,2,1,0:T(8,128)(2,1)S(1)} %pad_maximum_fusion.f0_ref), channel_id=1, source_target_pairs={{0,2},{2,4},{4,6},{6,0},{1,3},{3,5},{5,7},{7,1},{8,10},{10,12},{12... | collective-permute-start | bytes 786440 | tf_op jit(solution)/shard_map/ppermute | solution.py:187
  128.3 0.0 collective-permute-done.1.o2_ref
  128.3 0.0 collective-permute-done.o1_ref
  128.3 0.0 all-to-all-done.3.got_ref
  128.3 1.5 shard_map.106
  129.8 4.2 %all-to-all-start.4 = ((bf16[4,320,128]{2,1,0:T(8,128)(2,1)}), bf16[4,320,128]{2,1,0:T(8,128)(2,1)S(1)}, u32[]{:S(2)}, u32[]{:S(2)}) async-start(bf16[4,320,128]{2,1,0:T(8,128)(2,1)} %shard_map.106), calls=%async_computation.4 | async-start | bytes 655360 | tf_op jit(solution)/shard_map/all_to_all | solution.py:182
  134.0 0.0 collective-permute-done.9.f3_ref
  134.0 0.1 collective-permute-done.8.f2_ref
  134.1 2.7 %collective-permute-done.7.f1_ref = bf16[2,4,64,256]{3,2,1,0:T(8,128)(2,1)S(1)} collective-permute-done((bf16[2,4,64,256]{3,2,1,0:T(8,128)(2,1)S(1)}, bf16[2,4,64,256]{3,2,1,0:T(8,128)(2,1)S(1)}, u32[]{:S(2)}, u32[]{:S(2)}) %collective-permute-start.7) | collective-permute-done | bytes 262176 | tf_op jit(solution)/shard_map/ppermute | solution.py:187
  136.8 4.3 %all-to-all-done.4.got_ref = bf16[4,320,128]{2,1,0:T(8,128)(2,1)S(1)} async-done(((bf16[4,320,128]{2,1,0:T(8,128)(2,1)}), bf16[4,320,128]{2,1,0:T(8,128)(2,1)S(1)}, u32[]{:S(2)}, u32[]{:S(2)}) %all-to-all-start.4) | async-done | bytes 327712 | tf_op jit(solution)/shard_map/all_to_all | solution.py:182
  141.0 1.9 %shard_map.108 = (bf16[256,128]{1,0:T(8,128)(2,1)S(1)}, bf16[256,128]{1,0:T(8,128)(2,1)S(1)}, bf16[8,64,128]{2,1,0:T(8,128)(2,1)}) custom-call(s32[3]{0:T(128)} %pad_add_fusion.place_ref, bf16[4,320,128]{2,1,0:T(8,128)(2,1)S(1)} %all-to-all-done.4.got_ref, bf16[2,4,64,256]{3,2,1,0:T(8,128)(2,1)S(1)} %pad_maximum_fusion.f0_ref, ...), custom_call_target="tpu_custom_call" | custom-call | tf_op jit(solution)/shard_map/pallas_call | solution.py:168
  142.9 11.9 %all-to-all-start.5 = ((bf16[16,32,128]{2,1,0:T(8,128)(2,1)}), bf16[16,32,128]{2,1,0:T(8,128)(2,1)S(1)}, u32[]{:S(2)}, u32[]{:S(2)}) async-start(bf16[16,32,128]{2,1,0:T(8,128)(2,1)} %bitcast.21), calls=%async_computation.5 | async-start | bytes 262144 | tf_op jit(solution)/shard_map/all_to_all | solution.py:182
  154.9 0.6 copy.11
  155.5 0.6 copy.12
  156.1 0.6 copy.13
  156.8 11.3 %all-to-all-done.5 = bf16[16,32,128]{2,1,0:T(8,128)(2,1)S(1)} async-done(((bf16[16,32,128]{2,1,0:T(8,128)(2,1)}), bf16[16,32,128]{2,1,0:T(8,128)(2,1)S(1)}, u32[]{:S(2)}, u32[]{:S(2)}) %all-to-all-start.5) | async-done | bytes 131104 | tf_op jit(solution)/shard_map/all_to_all | solution.py:182
  168.1 0.6 convert_reduce_fusion
  (4 shorter events, 0.1 us)
Async XLA Ops:
  0.6 0.8 copy-start
  1.5 0.8 copy-start.2
  45.6 26.9 %copy-start.1 = (bf16[256,128]{1,0:T(8,128)(2,1)S(1)}, bf16[256,128]{1,0:T(8,128)(2,1)}, u32[]{:S(2)}) copy-start(bf16[256,128]{1,0:T(8,128)(2,1)} %keys_ref.3) | copy-start | bytes 196612
  45.6 26.9 %copy-start.3 = (bf16[256,128]{1,0:T(8,128)(2,1)S(1)}, bf16[256,128]{1,0:T(8,128)(2,1)}, u32[]{:S(2)}) copy-start(bf16[256,128]{1,0:T(8,128)(2,1)} %values_ref.3) | copy-start | bytes 196612
  45.6 26.9 %copy-start.5 = (bf16[256,128]{1,0:T(8,128)(2,1)S(1)}, bf16[256,128]{1,0:T(8,128)(2,1)}, u32[]{:S(2)}) copy-start(bf16[256,128]{1,0:T(8,128)(2,1)} %queries_ref.1) | copy-start | bytes 196612
  45.6 26.9 %copy-start.6 = (bf16[256,128]{1,0:T(8,128)(2,1)S(1)}, bf16[256,128]{1,0:T(8,128)(2,1)}, u32[]{:S(2)}) copy-start(bf16[256,128]{1,0:T(8,128)(2,1)} %grad_ref.1) | copy-start | bytes 196612
  45.6 26.9 %all-to-all-start.1 = ((bf16[64,16,128]{2,1,0:T(8,128)(2,1)}), bf16[64,16,128]{2,1,0:T(8,128)(2,1)S(1)}, u32[]{:S(2)}, u32[]{:S(2)}) async-start(bf16[64,16,128]{2,1,0:T(8,128)(2,1)} %bitcast.6), calls=%async_computation.1 | async-start | bytes 524288 | tf_op jit(solution)/shard_map/all_to_all | solution.py:182
  50.7 21.8 %copy-start.7 = (f32[2,256]{1,0:T(2,128)S(1)}, f32[2,256]{1,0:T(2,128)}, u32[]{:S(2)}) copy-start(f32[2,256]{1,0:T(2,128)} %sums_ref.1) | copy-start | bytes 6148
  75.4 4.8 %copy-start.4 = (bf16[256,256]{1,0:T(8,128)(2,1)S(1)}, bf16[256,256]{1,0:T(8,128)(2,1)}, u32[]{:S(2)}) copy-start(bf16[256,256]{1,0:T(8,128)(2,1)} %normed_ref.1) | copy-start | bytes 393220
  75.4 26.7 %all-to-all-start.2 = ((bf16[64,16,128]{2,1,0:T(8,128)(2,1)}), bf16[64,16,128]{2,1,0:T(8,128)(2,1)S(1)}, u32[]{:S(2)}, u32[]{:S(2)}) async-start(bf16[64,16,128]{2,1,0:T(8,128)(2,1)} %get-tuple-element.15), calls=%async_computation.2 | async-start | bytes 524288 | tf_op jit(solution)/shard_map/all_to_all | solution.py:182
  81.2 25.5 %collective-permute-start.5 = (bf16[64,256]{1,0:T(8,128)(2,1)S(1)}, bf16[64,256]{1,0:T(8,128)(2,1)S(1)}, u32[]{:S(2)}, u32[]{:S(2)}) collective-permute-start(bf16[64,256]{1,0:T(8,128)(2,1)S(1)} %get-tuple-element.23), channel_id=1, source_target_pairs={{0,24},{8,0},{16,8},{24,16},{1,25},{9,1},{17,9},{25,17},{2,26},{10... | collective-permute-start | bytes 98312 | tf_op jit(solution)/shard_map/ppermute | solution.py:187
  85.9 20.8 %collective-permute-start.4 = (bf16[64,256]{1,0:T(8,128)(2,1)S(1)}, bf16[64,256]{1,0:T(8,128)(2,1)S(1)}, u32[]{:S(2)}, u32[]{:S(2)}) collective-permute-start(bf16[64,256]{1,0:T(8,128)(2,1)S(1)} %get-tuple-element.24), channel_id=1, source_target_pairs={{0,16},{8,24},{16,0},{24,8},{1,17},{9,25},{17,1},{25,9},{2,18},{10... | collective-permute-start | bytes 98312 | tf_op jit(solution)/shard_map/ppermute | solution.py:187
  88.6 18.0 %collective-permute-start.3 = (bf16[64,256]{1,0:T(8,128)(2,1)S(1)}, bf16[64,256]{1,0:T(8,128)(2,1)S(1)}, u32[]{:S(2)}, u32[]{:S(2)}) collective-permute-start(bf16[64,256]{1,0:T(8,128)(2,1)S(1)} %get-tuple-element.25), channel_id=1, source_target_pairs={{0,8},{8,16},{16,24},{24,0},{1,9},{9,17},{17,25},{25,1},{2,10},{10... | collective-permute-start | bytes 98312 | tf_op jit(solution)/shard_map/ppermute | solution.py:187
  103.1 25.2 %all-to-all-start.3 = ((bf16[16,32,128]{2,1,0:T(8,128)(2,1)}), bf16[16,32,128]{2,1,0:T(8,128)(2,1)S(1)}, u32[]{:S(2)}, u32[]{:S(2)}) async-start(bf16[16,32,128]{2,1,0:T(8,128)(2,1)} %bitcast.8), calls=%async_computation.3 | async-start | bytes 262144 | tf_op jit(solution)/shard_map/all_to_all | solution.py:182
  106.7 10.9 %collective-permute-start.6 = (bf16[4,64,256]{2,1,0:T(8,128)(2,1)S(1)}, bf16[4,64,256]{2,1,0:T(8,128)(2,1)S(1)}, u32[]{:S(2)}, u32[]{:S(2)}) collective-permute-start(bf16[4,64,256]{2,1,0:T(8,128)(2,1)S(1)} %get-tuple-element.21), channel_id=1, source_target_pairs={{0,1},{1,0},{2,3},{3,2},{4,5},{5,4},{6,7},{7,6},{8,9},{9,8},{10,11... | collective-permute-start | bytes 393224 | tf_op jit(solution)/shard_map/ppermute | solution.py:187
  108.7 15.9 %collective-permute-start.2 = (bf16[2,64,128]{2,1,0:T(8,128)(2,1)S(1)}, bf16[2,64,128]{2,1,0:T(8,128)(2,1)S(1)}, u32[]{:S(2)}, u32[]{:S(2)}) collective-permute-start(bf16[2,64,128]{2,1,0:T(8,128)(2,1)S(1)} %get-tuple-element.26), channel_id=1, source_target_pairs={{0,24},{8,0},{16,8},{24,16},{1,25},{9,1},{17,9},{25,17},{2,26},{10... | collective-permute-start | bytes 98312 | tf_op jit(solution)/shard_map/ppermute | solution.py:187
  112.1 16.2 %collective-permute-start.1 = (bf16[2,64,128]{2,1,0:T(8,128)(2,1)S(1)}, bf16[2,64,128]{2,1,0:T(8,128)(2,1)S(1)}, u32[]{:S(2)}, u32[]{:S(2)}) collective-permute-start(bf16[2,64,128]{2,1,0:T(8,128)(2,1)S(1)} %get-tuple-element.27), channel_id=1, source_target_pairs={{0,16},{8,24},{16,0},{24,8},{1,17},{9,25},{17,1},{25,9},{2,18},{10... | collective-permute-start | bytes 98312 | tf_op jit(solution)/shard_map/ppermute | solution.py:187
  115.3 13.0 %collective-permute-start = (bf16[2,64,128]{2,1,0:T(8,128)(2,1)S(1)}, bf16[2,64,128]{2,1,0:T(8,128)(2,1)S(1)}, u32[]{:S(2)}, u32[]{:S(2)}) collective-permute-start(bf16[2,64,128]{2,1,0:T(8,128)(2,1)S(1)} %get-tuple-element.28), channel_id=1, source_target_pairs={{0,8},{8,16},{16,24},{24,0},{1,9},{9,17},{17,25},{25,1},{2,10},{10... | collective-permute-start | bytes 98312 | tf_op jit(solution)/shard_map/ppermute | solution.py:187
  117.7 16.3 %collective-permute-start.9 = (bf16[2,4,64,256]{3,2,1,0:T(8,128)(2,1)S(1)}, bf16[2,4,64,256]{3,2,1,0:T(8,128)(2,1)S(1)}, u32[]{:S(2)}, u32[]{:S(2)}) collective-permute-start(bf16[2,4,64,256]{3,2,1,0:T(8,128)(2,1)S(1)} %pad_maximum_fusion.f0_ref), channel_id=1, source_target_pairs={{0,6},{2,0},{4,2},{6,4},{1,7},{3,1},{5,3},{7,5},{8,14},{10,8},{12,... | collective-permute-start | bytes 786440 | tf_op jit(solution)/shard_map/ppermute | solution.py:187
  120.2 13.9 %collective-permute-start.8 = (bf16[2,4,64,256]{3,2,1,0:T(8,128)(2,1)S(1)}, bf16[2,4,64,256]{3,2,1,0:T(8,128)(2,1)S(1)}, u32[]{:S(2)}, u32[]{:S(2)}) collective-permute-start(bf16[2,4,64,256]{3,2,1,0:T(8,128)(2,1)S(1)} %pad_maximum_fusion.f0_ref), channel_id=1, source_target_pairs={{0,4},{2,6},{4,0},{6,2},{1,5},{3,7},{5,1},{7,3},{8,12},{10,14},{12... | collective-permute-start | bytes 786440 | tf_op jit(solution)/shard_map/ppermute | solution.py:187
  124.6 12.2 %collective-permute-start.7 = (bf16[2,4,64,256]{3,2,1,0:T(8,128)(2,1)S(1)}, bf16[2,4,64,256]{3,2,1,0:T(8,128)(2,1)S(1)}, u32[]{:S(2)}, u32[]{:S(2)}) collective-permute-start(bf16[2,4,64,256]{3,2,1,0:T(8,128)(2,1)S(1)} %pad_maximum_fusion.f0_ref), channel_id=1, source_target_pairs={{0,2},{2,4},{4,6},{6,0},{1,3},{3,5},{5,7},{7,1},{8,10},{10,12},{12... | collective-permute-start | bytes 786440 | tf_op jit(solution)/shard_map/ppermute | solution.py:187
  129.8 11.2 %all-to-all-start.4 = ((bf16[4,320,128]{2,1,0:T(8,128)(2,1)}), bf16[4,320,128]{2,1,0:T(8,128)(2,1)S(1)}, u32[]{:S(2)}, u32[]{:S(2)}) async-start(bf16[4,320,128]{2,1,0:T(8,128)(2,1)} %shard_map.106), calls=%async_computation.4 | async-start | bytes 655360 | tf_op jit(solution)/shard_map/all_to_all | solution.py:182
  142.9 25.1 %all-to-all-start.5 = ((bf16[16,32,128]{2,1,0:T(8,128)(2,1)}), bf16[16,32,128]{2,1,0:T(8,128)(2,1)S(1)}, u32[]{:S(2)}, u32[]{:S(2)}) async-start(bf16[16,32,128]{2,1,0:T(8,128)(2,1)} %bitcast.21), calls=%async_computation.5 | async-start | bytes 262144 | tf_op jit(solution)/shard_map/all_to_all | solution.py:182
